TPU v7x, 32 devices: a whole 2x2x4 slice. The times are simulated.
32 devices in a mesh: ep: 4 (over y, x), tp: 8 (over z, core).
Axes of the slice: x: 2, y: 2, z: 4, core: 2. Of those that a mesh axis runs over, the one named last changes fastest.
Arguments:
- tokens: bfloat16 [256, 4096], P(('ep', 'tp')), may hold values from -6 to 6
- rec_state: float32 [256, 2048], P('ep', 'tp'), may hold values from -40 to 40
- conv_state: bfloat16 [256, 3, 2048], P('ep', None, 'tp'), may hold values from -6 to 6
- route_ids: int32 [256, 4], P('ep'), may hold values from 0 to 15, all different within a row; in each aligned block of 8 rows (0 to 7, 8 to 15, ...) at most 2 rows name the same one
- route_weights: float32 [256, 4], P(('ep', 'tp')), may hold values from 0.1 to 1
- first_gain: bfloat16 [4096], replicated, may hold values from 0.099609375 to 1.8984375
- proj_input: bfloat16 [4096, 2048], P(None, 'tp'), may hold values from -0.09375 to 0.09375
- proj_gate: bfloat16 [4096, 2048], P(None, 'tp'), may hold values from -0.09375 to 0.09375
- conv_taps: bfloat16 [4, 2048], replicated, may hold values from -1.5 to 1.5
- decay_logit: float32 [2048], replicated, may hold values from 1 to 6
- block_decay: bfloat16 [16, 128, 128], replicated, may hold values from -0.5 to 0.5
- block_input: bfloat16 [16, 128, 128], replicated, may hold values from -0.5 to 0.5
- rec_gain: bfloat16 [2048], replicated, may hold values from 0.099609375 to 1.8984375
- proj_out: bfloat16 [2048, 4096], P('tp'), may hold values from -0.125 to 0.125
- second_gain: bfloat16 [4096], replicated, may hold values from 0.099609375 to 1.8984375
- expert_gate: bfloat16 [16, 4096, 4096], P('ep', None, 'tp'), may hold values from -0.21875 to 0.21875
- expert_up: bfloat16 [16, 4096, 4096], P('ep', None, 'tp'), may hold values from -0.21875 to 0.21875
- expert_down: bfloat16 [16, 4096, 4096], P('ep', 'tp'), may hold values from -0.0234375 to 0.0234375
Outputs:
- result: bfloat16 [256, 4096], P(('ep', 'tp'))
- new_state: float32 [256, 2048], P('ep', 'tp')
- new_conv: bfloat16 [256, 3, 2048], P('ep', None, 'tp')
Inputs may be any that keep to these rules, and one draw needn't show every extreme that they name: `route_ids`: each row names 4 different experts; in the rows of one device (aligned blocks of 8 rows) no expert is named by more than 2 rows, and one is named by exactly 2.
All inputs are finite; a program needn't handle non-finite values.
Results may differ from a plain program's by a relative error of at most 0.025.
Values may be sent and summed in bfloat16 or wider, within the bound.
A program may use at most 128 MiB of HBM per device.

v0:
```python
import jax
import jax.numpy as jnp
from jax import lax
from jax.sharding import PartitionSpec as P

EXPERTS = 16
EPS = 1e-06
CLAMP = 7.0
ALPHA = 1.702
RATE = 8.0


def norm_rows(values, gain):
    scale = lax.rsqrt(jnp.mean(values * values, axis=-1, keepdims=True) + EPS)
    return values * scale * gain.astype(jnp.float32)


def slot_positions(ids, blocks):
    rows, picks = ids.shape
    onehot = (ids[:, :, None] == jnp.arange(EXPERTS, dtype=jnp.int32)).astype(jnp.int32)
    onehot = onehot.reshape(blocks, rows // blocks * picks, EXPERTS)
    before = jnp.cumsum(onehot, axis=1) - onehot
    return jnp.sum(before * onehot, axis=-1).reshape(rows, picks)


def dispatch_rows(slots, rows_in, total):
    hits = (slots[:, :, None] == jnp.arange(total, dtype=jnp.int32)).astype(jnp.bfloat16)
    chooser = jnp.sum(hits, axis=1)
    return jnp.einsum("ns,nd->sd", chooser, rows_in, preferred_element_type=jnp.float32).astype(
        jnp.bfloat16
    )


def run_experts(piece, expert_gate, expert_up, expert_down):
    gate = jnp.einsum("erd,edf->erf", piece, expert_gate, preferred_element_type=jnp.float32)
    upper = jnp.einsum("erd,edf->erf", piece, expert_up, preferred_element_type=jnp.float32)
    clipped = jnp.minimum(gate, CLAMP)
    act = (
        (jnp.clip(upper, -CLAMP, CLAMP) + 1.0) * (clipped * jax.nn.sigmoid(ALPHA * clipped))
    ).astype(jnp.bfloat16)
    return jnp.einsum("erf,efd->erd", act, expert_down, preferred_element_type=jnp.float32)


def per_device(
    tokens,
    rec_state,
    conv_state,
    route_ids,
    route_weights,
    first_gain,
    proj_input,
    proj_gate,
    conv_taps,
    decay_logit,
    block_decay,
    block_input,
    rec_gain,
    proj_out,
    second_gain,
    expert_gate,
    expert_up,
    expert_down,
):
    tp_count = lax.axis_size("tp")
    tp_place = lax.axis_index("tp")
    local_width = proj_input.shape[1]
    seq_count = rec_state.shape[0]
    own_count = tokens.shape[0]
    top_count = route_ids.shape[1]
    capacity = max(2, own_count * top_count // EXPERTS)
    first_channel = tp_place * local_width
    own_values = tokens.astype(jnp.float32)
    normed = norm_rows(own_values, first_gain).astype(jnp.bfloat16)
    piece = lax.all_gather(normed, "tp", axis=0, tiled=True)
    both = jnp.concatenate(
        [
            jnp.dot(piece, proj_input, preferred_element_type=jnp.float32),
            jnp.dot(piece, proj_gate, preferred_element_type=jnp.float32),
        ],
        axis=1,
    )
    joined = both.astype(jnp.bfloat16)
    branch_in = joined[:, :local_width]
    branch_gate = joined[:, local_width:]
    tap_weights = lax.dynamic_slice_in_dim(conv_taps, first_channel, local_width, 1).astype(
        jnp.float32
    )
    conv_values = conv_state.astype(jnp.float32)
    conv_output = tap_weights[-1] * branch_in.astype(jnp.float32)
    for tap in range(conv_state.shape[1]):
        conv_output = conv_output + tap_weights[tap] * conv_values[:, tap]
    new_conv = jnp.concatenate([conv_state[:, 1:], branch_in[:, None, :]], axis=1)
    block_width = block_decay.shape[1]
    local_blocks = local_width // block_width
    decay_mats = lax.dynamic_slice_in_dim(block_decay, tp_place * local_blocks, local_blocks, 0)
    input_mats = lax.dynamic_slice_in_dim(block_input, tp_place * local_blocks, local_blocks, 0)
    blocked = conv_output.astype(jnp.bfloat16).reshape(seq_count, local_blocks, block_width)
    decay_gate = jax.nn.sigmoid(
        jnp.einsum("rnk,nkj->rnj", blocked, decay_mats, preferred_element_type=jnp.float32).reshape(
            seq_count, local_width
        )
    )
    input_gate = jax.nn.sigmoid(
        jnp.einsum("rnk,nkj->rnj", blocked, input_mats, preferred_element_type=jnp.float32).reshape(
            seq_count, local_width
        )
    )
    decay_logits = lax.dynamic_slice_in_dim(decay_logit, first_channel, local_width, 0)
    log_keep = -RATE * decay_gate * jax.nn.softplus(-decay_logits)
    keep_factor = jnp.exp(log_keep)
    fresh_input = jnp.sqrt(-jnp.expm1(2.0 * log_keep)) * input_gate * conv_output
    new_state = keep_factor * rec_state + fresh_input
    hidden = new_state * jax.nn.gelu(branch_gate.astype(jnp.float32))
    squares = jnp.sum(hidden * hidden, axis=1, keepdims=True)
    gain_part = lax.dynamic_slice_in_dim(rec_gain, first_channel, local_width, 0).astype(
        jnp.float32
    )
    partial_value = jnp.dot(
        (hidden * gain_part).astype(jnp.bfloat16), proj_out, preferred_element_type=jnp.float32
    )
    channels = local_width * tp_count
    width_out = proj_out.shape[1]
    own_ids = lax.dynamic_slice_in_dim(route_ids, tp_place * own_count, own_count, 0)
    own_slots = own_ids * capacity + slot_positions(own_ids, 1)
    mix_part, own_squares = (
        lax.psum_scatter(
            partial_value.astype(jnp.bfloat16), "tp", scatter_dimension=0, tiled=True
        ).astype(jnp.float32),
        lax.psum_scatter(
            squares.astype(jnp.bfloat16), "tp", scatter_dimension=0, tiled=True
        ).astype(jnp.float32),
    )
    residual = own_values + mix_part * lax.rsqrt(own_squares / channels + EPS)
    second_normed = norm_rows(residual, second_gain).astype(jnp.bfloat16)
    outgoing = dispatch_rows(own_slots, second_normed, EXPERTS * capacity).reshape(
        EXPERTS, capacity, width_out
    )
    arrived = lax.all_to_all(outgoing, "ep", split_axis=0, concat_axis=1, tiled=True)
    partials = run_experts(
        lax.all_gather(arrived, "tp", axis=1, tiled=True), expert_gate, expert_up, expert_down
    )
    summed_rows = lax.psum_scatter(
        partials.astype(jnp.bfloat16), "tp", scatter_dimension=1, tiled=True
    )
    returned = lax.all_to_all(summed_rows, "ep", split_axis=1, concat_axis=0, tiled=True)
    returned_rows = returned.reshape(EXPERTS * capacity, width_out).astype(jnp.float32)
    slot_hits = (own_slots[:, :, None] == jnp.arange(EXPERTS * capacity, dtype=jnp.int32)).astype(
        jnp.float32
    )
    combine_weights = jnp.sum(slot_hits * route_weights[:, :, None], axis=1)
    expert_mix = jnp.dot(combine_weights, returned_rows, precision=lax.Precision.HIGHEST)
    result = (residual + expert_mix).astype(jnp.bfloat16)
    return (result, new_state, new_conv)


def solution(mesh):
    in_specs = (
        P(("ep", "tp"), None),
        P("ep", "tp"),
        P("ep", None, "tp"),
        P("ep", None),
        P(("ep", "tp"), None),
        P(),
        P(None, "tp"),
        P(None, "tp"),
        P(),
        P(),
        P(),
        P(),
        P(),
        P("tp", None),
        P(),
        P("ep", None, "tp"),
        P("ep", None, "tp"),
        P("ep", "tp", None),
    )
    out_specs = (P(("ep", "tp"), None), P("ep", "tp"), P("ep", None, "tp"))
    return jax.shard_map(
        per_device, mesh=mesh, in_specs=in_specs, out_specs=out_specs, check_vma=False
    )
```

profile of v0, /device:TPU:0, one launch (start us, length us, event | category | flops | bytes accessed | tf_op | source)
XLA Modules:
  0.0 196.3 jit_solution(4809331061785495694)
XLA Ops:
  7.2 0.8 dynamic-slice_convert_fusion
  8.1 0.7 convert_element_type.98
  8.8 1.0 fusion.17
  9.8 0.9 fusion.19
  10.7 16.5 %all_gather.6 = bf16[64,4096]{1,0:T(8,128)(2,1)S(1)} all-gather(bf16[8,4096]{1,0:T(8,128)(2,1)S(1)} %fusion.19), channel_id=1, replica_groups=mesh['ep'=4,'tp'=8] {'tp'}, dimensions={0}, use_global_device_ids=true | all-gather | bytes 589824 | tf_op jit(solution)/shard_map/all_gather | solution.py:74
  27.2 0.9 convert_element_type.101
  28.1 2.1 %convolution_convert_fusion.4 = bf16[64,256]{1,0:T(8,128)(2,1)S(1)} fusion(bf16[64,4096]{1,0:T(8,128)(2,1)S(1)} %all_gather.6, bf16[4096,256]{1,0:T(8,128)(2,1)} %param.24), kind=kOutput, calls=%fused_computation.22 | convolution fusion | flops 134234112 | bytes 2654208 | tf_op jit(solution)/shard_map/dot_general | solution.py:77
  30.2 1.0 fusion.11
  31.2 1.0 fusion.7
  32.2 0.8 fusion.49
  33.0 0.8 dynamic-slice_convert_fusion.2
  33.9 2.2 %multiply_reduce_fusion.1 = (bf16[64]{0:T(256)(128)(2,1)S(1)}, f32[64,256]{1,0:T(8,128)S(1)}) fusion(f32[64,256]{1,0:T(8,128)S(1)} %fusion.29, bf16[64,4096]{1,0:T(8,128)(2,1)S(1)} %all_gather.6, bf16[4096,256]{1,0:T(8,128)(2,1)} %param.25), kind=kOutput, calls=%fused_computation.63 | convolution fusion | flops 134430656 | bytes 2752640 | tf_op jit(solution)/shard_map/dot_general | solution.py:78
  36.1 1.3 convolution_convert_fusion.1
  38.3 0.6 dynamic-slice
  39.5 17.0 %all-reduce = bf16[64,1]{0,1:T(2,128)(2,1)S(1)} all-reduce(bf16[64,1]{0,1:T(2,128)(2,1)S(1)} %bitcast.97), channel_id=3, replica_groups=mesh['ep'=4,'tp'=8] {'tp'}, use_global_device_ids=true, to_apply=%region_3.4.clone | all-reduce | flops 64 | bytes 256
  56.6 13.2 %reduce-scatter.6.cloned.1.call-done = bf16[8,4096]{1,0:T(8,128)(2,1)} async-done(((bf16[64,4096]{1,0:T(8,128)(2,1)}), bf16[8,4096]{1,0:T(8,128)(2,1)}) %reduce-scatter.6.cloned.1.call-update) | async-done | bytes 65552 | tf_op jit(solution)/shard_map/reduce_scatter | solution.py:126
  69.9 1.1 multiply_reduce_fusion
  71.0 1.1 convolution_convert_fusion.2
  72.3 9.2 %all_to_all.33 = bf16[16,2,4096]{2,1,0:T(2,128)(2,1)S(1)} all-to-all(bf16[16,2,4096]{2,1,0:T(2,128)(2,1)S(1)} %reshape.161), channel_id=1, replica_groups=mesh['ep'=4,'tp'=8] {'ep'}, dimensions={0} | all-to-all | bytes 524288 | tf_op jit(solution)/shard_map/all_to_all | solution.py:138
  81.7 0.8 all_to_all.27
  82.7 26.3 %all-gather.2.cloned.1.call-done = bf16[4,64,4096]{2,1,0:T(8,128)(2,1)} async-done(((bf16[4,8,4096]{2,1,0:T(8,128)(2,1)}), bf16[4,64,4096]{2,1,0:T(8,128)(2,1)}) %all-gather.2.cloned.1.call-update) | async-done | bytes 2097168 | tf_op jit(solution)/shard_map/all_gather | solution.py:140
  109.0 9.5 %convolution_minimum_fusion = f32[4,64,512]{2,1,0:T(8,128)S(1)} fusion(bf16[4,64,4096]{2,1,0:T(8,128)(2,1)} %all-gather.2.cloned.1.call-done, bf16[4,4096,512]{2,1,0:T(8,128)(2,1)} %param.33), kind=kOutput, calls=%fused_computation.5 | convolution fusion | flops 1073872896 | bytes 19398656 | tf_op jit(solution)/shard_map/erd,edf->erf/dot_general | solution.py:35
  118.6 17.8 %convolution_convert_fusion = bf16[4,64,4096]{2,1,0:T(8,128)(2,1)} fusion(bf16[4,512,4096]{2,1,0:T(8,128)(2,1)} %param.35, bf16[4,64,4096]{2,1,0:T(8,128)(2,1)S(1)} %copy-done.2, bf16[4,4096,512]{2,1,0:T(8,128)(2,1)} %param.34, f32[4,64,512]{2,1,0:T(8,128)S(1)} %convolution_minimum_fusion), kind=kOutput, calls=%fused_computation | convolution fusion | flops 2149711872 | bytes 38273024 | tf_op jit(solution)/shard_map/erf,efd->erd/dot_general | solution.py:41
  136.4 3.2 %copy.56 = bf16[4,64,4096]{2,0,1:T(4,128)(2,1)S(1)} copy(bf16[4,64,4096]{2,1,0:T(8,128)(2,1)} %convolution_convert_fusion) | data formatting | bytes 4194304
  139.6 2.6 %copy.62 = bf16[8,8,4,4096]{3,1,2,0:T(8,128)(2,1)} copy(bf16[8,8,4,4096]{3,2,1,0:T(4,128)(2,1)S(1)} %bitcast.87) | data formatting | bytes 4194304
  142.2 35.6 %reduce-scatter.8.cloned.1.call-done = bf16[8,16384]{1,0:T(8,128)(2,1)} async-done(((bf16[64,16384]{1,0:T(8,128)(2,1)}), bf16[8,16384]{1,0:T(8,128)(2,1)}) %reduce-scatter.8.cloned.1.call-update) | async-done | bytes 262160
  177.8 1.8 reshape.166
  179.6 3.5 %all-to-all-start.1 = ((bf16[4,8,4096]{2,0,1:T(4,128)(2,1)}), bf16[4,8,4096]{2,0,1:T(4,128)(2,1)S(1)}, u32[]{:S(2)}, u32[]{:S(2)}) async-start(bf16[4,8,4096]{2,0,1:T(4,128)(2,1)} %bitcast.19), calls=%async_computation.2 | async-start | bytes 524288 | tf_op jit(solution)/shard_map/all_to_all | solution.py:145
  183.1 0.7 pad_maximum_fusion
  183.9 4.6 %all-to-all-done.1 = bf16[4,8,4096]{2,0,1:T(4,128)(2,1)S(1)} async-done(((bf16[4,8,4096]{2,0,1:T(4,128)(2,1)}), bf16[4,8,4096]{2,0,1:T(4,128)(2,1)S(1)}, u32[]{:S(2)}, u32[]{:S(2)}) %all-to-all-start.1) | async-done | bytes 262176 | tf_op jit(solution)/shard_map/all_to_all | solution.py:145
  188.5 0.3 copy.77
  188.9 0.9 fusion
  (51 shorter events, 2.0 us)
Async XLA Ops:
  7.2 29.0 %copy-start = (bf16[256,4096]{1,0:T(8,128)(2,1)S(1)}, bf16[256,4096]{1,0:T(8,128)(2,1)}, u32[]{:S(2)}) copy-start(bf16[256,4096]{1,0:T(8,128)(2,1)} %param.31) | copy-start | bytes 6291460
  7.2 62.7 %reduce-scatter.6.cloned.1.call-start = ((), (), s32[]{:S(2)}) async-start(), calls=%async_computation.4 | async-start | bytes 589824 | tf_op jit(solution)/shard_map/reduce_scatter | solution.py:126
  27.2 6.6 %copy-start.6 = (f32[64,256]{1,0:T(8,128)S(1)}, f32[64,256]{1,0:T(8,128)}, u32[]{:S(2)}) copy-start(f32[64,256]{1,0:T(8,128)} %param.19) | copy-start | bytes 196612
  33.9 3.6 %copy-start.5 = (f32[64,256]{1,0:T(8,128)}, f32[64,256]{1,0:T(8,128)S(1)}, u32[]{:S(2)}) copy-start(f32[64,256]{1,0:T(8,128)S(1)} %fusion.29) | copy-start | bytes 196612
  36.1 1.4 copy-start.8
  36.1 2.1 %copy-start.7 = (bf16[4096]{0:T(1024)(128)(2,1)S(1)}, bf16[4096]{0:T(1024)(128)(2,1)}, u32[]{:S(2)}) copy-start(bf16[4096]{0:T(1024)(128)(2,1)} %param.32) | copy-start | bytes 24580
  36.1 2.1 %copy-start.10 = (u32[32]{0:T(128)S(1)}, u32[32]{0:T(128)}, u32[]{:S(2)}) copy-start(u32[32]{0:T(128)} %constant.63) | copy-start | bytes 388
  36.1 33.8 %copy-start.3 = (bf16[8,4096]{1,0:T(8,128)(2,1)S(1)}, bf16[8,4096]{1,0:T(8,128)(2,1)}, u32[]{:S(2)}) copy-start(bf16[8,4096]{1,0:T(8,128)(2,1)} %param.18) | copy-start | bytes 196612
  37.4 71.6 %all-gather.2.cloned.1.call-start = ((), (), s32[]{:S(2)}) async-start(), calls=%async_computation.5 | async-start | bytes 2359296 | tf_op jit(solution)/shard_map/all_gather | solution.py:140
  82.5 95.3 %reduce-scatter.8.cloned.1.call-start = ((), (), s32[]{:S(2)}) async-start(), calls=%async_computation.6 | async-start | bytes 2359296
  109.0 9.5 %copy-start.2 = (bf16[4,64,4096]{2,1,0:T(8,128)(2,1)S(1)}, bf16[4,64,4096]{2,1,0:T(8,128)(2,1)}, u32[]{:S(2)}) copy-start(bf16[4,64,4096]{2,1,0:T(8,128)(2,1)} %all-gather.2.cloned.1.call-done) | copy-start | bytes 6291460
  142.1 41.0 %slice-start = ((bf16[64,3,256]{2,0,1:T(8,128)(2,1)}), bf16[64,2,256]{2,0,1:T(8,128)(2,1)S(1)}, s32[]{:S(2)}) async-start(bf16[64,3,256]{2,0,1:T(8,128)(2,1)} %param.20), calls=%async_computation.7 | async-start | bytes 131072 | tf_op jit(solution)/shard_map/slice | solution.py:92
  142.1 41.6 %copy-start.9 = (f32[8,4]{0,1:T(4,128)S(1)}, f32[8,4]{0,1:T(4,128)}, u32[]{:S(2)}) copy-start(f32[8,4]{0,1:T(4,128)} %param.22) | copy-start | bytes 388
  142.1 47.6 %copy-start.1 = (bf16[256,4096]{1,0:T(8,128)(2,1)S(1)}, bf16[256,4096]{1,0:T(8,128)(2,1)}, u32[]{:S(2)}) copy-start(bf16[256,4096]{1,0:T(8,128)(2,1)} %param.31) | copy-start | bytes 6291460
  142.1 46.7 %copy-start.4 = (bf16[8,4096]{1,0:T(8,128)(2,1)S(1)}, bf16[8,4096]{1,0:T(8,128)(2,1)}, u32[]{:S(2)}) copy-start(bf16[8,4096]{1,0:T(8,128)(2,1)} %reduce-scatter.6.cloned.1.call-done) | copy-start | bytes 196612
  179.6 8.9 %all-to-all-start.1 = ((bf16[4,8,4096]{2,0,1:T(4,128)(2,1)}), bf16[4,8,4096]{2,0,1:T(4,128)(2,1)S(1)}, u32[]{:S(2)}, u32[]{:S(2)}) async-start(bf16[4,8,4096]{2,0,1:T(4,128)(2,1)} %bitcast.19), calls=%async_computation.2 | async-start | bytes 524288 | tf_op jit(solution)/shard_map/all_to_all | solution.py:145
Sparse Core Ops, SparseCore 0:
  37.6 32.2 reduce-scatter.5
  82.6 26.3 all-gather.1
  142.3 35.4 reduce-scatter.7
where the time goes:
time: 197 us; the launch traced here: 196 us
  waiting for transfers between devices  79.8 us (41%)
  blocking collectives  42.7 us (22%)
  matrix products  36.8 us (19%)
  between operations  14.6 us (7%)
  local copies, waits for them, and re-layouts  10.3 us (5%)
  other arithmetic  8.29 us (4%)
  starting transfers between devices  3.84 us (2%)
    unnamed x4, waiting for transfers between devices  35.6 us
    all_gather x1, waiting for transfers between devices, per_device(): lax.all_gather(arrived, 'tp', axis=1, tiled=True)  26.3 us
    dot_general x1, matrix products, run_experts(): jnp.einsum('erf,efd->erd', act, expert_down, preferred_element_type=jnp.f...  17.8 us
    unnamed x1, blocking collectives  17 us
    all_gather x1, blocking collectives, per_device(): piece = lax.all_gather(normed, 'tp', axis=0, tiled=True)  16.5 us
    reduce_scatter x1, waiting for transfers between devices, per_device(): lax.psum_scatter(partial_value.astype(jnp.bfloat16), 'tp', scatter_dimens...  13.2 us
    dot_general x1, matrix products, run_experts(): jnp.einsum('erd,edf->erf', piece, expert_gate, preferred_element_type=jnp...  9.51 us
    all_to_all x1, blocking collectives, per_device(): lax.all_to_all(outgoing, 'ep', split_axis=0, concat_axis=1, tiled=True)  9.19 us
  transfers between devices with their start and end apart: 4, of which 4 were waited for; matrix products, arithmetic and copies ran while one was open for 1% of the time, Pallas kernels for 0%

commit v1 on v0

--- a/solution.py
+++ b/solution.py
@@ -137,7 +137,12 @@
     )
     arrived = lax.all_to_all(outgoing, "ep", split_axis=0, concat_axis=1, tiled=True)
     partials = run_experts(
-        lax.all_gather(arrived, "tp", axis=1, tiled=True), expert_gate, expert_up, expert_down
+        jnp.concatenate(
+            lax.all_to_all(jnp.stack([arrived] * lax.axis_size("tp")), "tp", 0, 0), axis=1
+        ),
+        expert_gate,
+        expert_up,
+        expert_down,
     )
     summed_rows = lax.psum_scatter(
         partials.astype(jnp.bfloat16), "tp", scatter_dimension=1, tiled=True

time: 197 us -> 219 us (1.11)
  blocking collectives: 42.7 us -> 94.2 us
  waiting for transfers between devices: 79.8 us -> 51.5 us
    all_to_all x0 -> x1, blocking collectives: none -> 51.5 us  [per_device(): lax.all_to_all(jnp.stack([arrived] * lax.axis_size('tp')), 'tp', 0, 0)]
    all_gather x1 -> x0, waiting for transfers between devices: 26.3 us -> none  [per_device(): lax.all_gather(arrived, 'tp', axis=1, tiled=True)]
    unnamed x4 -> x3, waiting for transfers between devices: 35.6 us -> 33.6 us
    unnamed x27 -> x25, local copies, waits for them, and re-layouts: 8.35 us -> 8.35 us
  transfers between devices with their start and end apart: 4 -> 3, of which waited for: 4 -> 3; matrix products, arithmetic and copies ran while one was open for 1% -> 1% of each run, Pallas kernels for 0% -> 0%
where the time goes in v1:
time: 219 us; the launch traced here: 218 us
  blocking collectives  94.2 us (43%)
  waiting for transfers between devices  51.5 us (24%)
  matrix products  36 us (16%)
  between operations  14.9 us (7%)
  local copies, waits for them, and re-layouts  9.82 us (4%)
  other arithmetic  8.29 us (4%)
  starting transfers between devices  3.6 us (2%)
    all_to_all x1, blocking collectives, per_device(): lax.all_to_all(jnp.stack([arrived] * lax.axis_size('tp')), 'tp', 0, 0)  51.5 us
    unnamed x3, waiting for transfers between devices  33.6 us
    dot_general x1, matrix products, run_experts(): jnp.einsum('erf,efd->erd', act, expert_down, preferred_element_type=jnp.f...  17.8 us
    unnamed x1, blocking collectives  17 us
    all_gather x1, blocking collectives, per_device(): piece = lax.all_gather(normed, 'tp', axis=0, tiled=True)  16.5 us
    reduce_scatter x1, waiting for transfers between devices, per_device(): lax.psum_scatter(partial_value.astype(jnp.bfloat16), 'tp', scatter_dimens...  13.2 us
    all_to_all x1, blocking collectives, per_device(): lax.all_to_all(outgoing, 'ep', split_axis=0, concat_axis=1, tiled=True)  9.19 us
    dot_general x1, matrix products, run_experts(): jnp.einsum('erd,edf->erf', piece, expert_gate, preferred_element_type=jnp...  8.73 us
  transfers between devices with their start and end apart: 3, of which 3 were waited for; matrix products, arithmetic and copies ran while one was open for 1% of the time, Pallas kernels for 0%

profile of v1, /device:TPU:0, one launch (start us, length us, event | category | flops | bytes accessed | tf_op | source)
XLA Modules:
  0.0 218.3 jit_solution(18004184634365336270)
XLA Ops:
  7.2 0.8 dynamic-slice_convert_fusion
  8.1 0.7 convert_element_type.98
  8.8 1.0 fusion.37
  9.8 0.9 fusion.39
  10.7 16.5 %all_gather.3 = bf16[64,4096]{1,0:T(8,128)(2,1)S(1)} all-gather(bf16[8,4096]{1,0:T(8,128)(2,1)S(1)} %fusion.39), channel_id=1, replica_groups=mesh['ep'=4,'tp'=8] {'tp'}, dimensions={0}, use_global_device_ids=true | all-gather | bytes 589824 | tf_op jit(solution)/shard_map/all_gather | solution.py:74
  27.2 0.9 convert_element_type.101
  28.1 2.1 convolution_convert_fusion.4
  30.2 1.0 fusion.25
  31.2 1.0 fusion.29
  32.2 0.8 fusion.69
  33.0 0.8 dynamic-slice_convert_fusion.2
  33.9 2.2 %multiply_reduce_fusion.1 = (bf16[64]{0:T(256)(128)(2,1)S(1)}, f32[64,256]{1,0:T(8,128)S(1)}) fusion(f32[64,256]{1,0:T(8,128)S(1)} %fusion.49, bf16[64,4096]{1,0:T(8,128)(2,1)S(1)} %all_gather.3, bf16[4096,256]{1,0:T(8,128)(2,1)} %param.25), kind=kOutput, calls=%fused_computation.68 | convolution fusion | flops 134430656 | bytes 2752640 | tf_op jit(solution)/shard_map/dot_general | solution.py:78
  36.1 1.3 convolution_convert_fusion.1
  38.3 0.6 dynamic-slice
  39.5 17.0 %all-reduce = bf16[64,1]{0,1:T(2,128)(2,1)S(1)} all-reduce(bf16[64,1]{0,1:T(2,128)(2,1)S(1)} %bitcast.120), channel_id=3, replica_groups=mesh['ep'=4,'tp'=8] {'tp'}, use_global_device_ids=true, to_apply=%region_3.4.clone | all-reduce | flops 64 | bytes 256
  56.6 13.2 %reduce-scatter.6.cloned.1.call-done = bf16[8,4096]{1,0:T(8,128)(2,1)} async-done(((bf16[64,4096]{1,0:T(8,128)(2,1)}), bf16[8,4096]{1,0:T(8,128)(2,1)}) %reduce-scatter.6.cloned.1.call-update) | async-done | bytes 65552 | tf_op jit(solution)/shard_map/reduce_scatter | solution.py:126
  69.9 1.1 multiply_reduce_fusion
  71.0 1.1 convolution_convert_fusion.2
  72.3 9.2 %all_to_all.35 = bf16[16,2,4096]{2,1,0:T(2,128)(2,1)S(1)} all-to-all(bf16[16,2,4096]{2,1,0:T(2,128)(2,1)S(1)} %reshape.170), channel_id=1, replica_groups=mesh['ep'=4,'tp'=8] {'ep'}, dimensions={0} | all-to-all | bytes 524288 | tf_op jit(solution)/shard_map/all_to_all | solution.py:138
  81.8 0.2 stack.5
  82.1 51.5 %all_to_all.36 = bf16[8,4,8,4096]{3,2,1,0:T(8,128)(2,1)S(1)} all-to-all(bf16[8,4,8,4096]{3,2,1,0:T(8,128)(2,1)S(1)} %stack.5), channel_id=1, replica_groups=mesh['ep'=4,'tp'=8] {'tp'}, dimensions={0} | all-to-all | bytes 4194304 | tf_op jit(solution)/shard_map/all_to_all | solution.py:141
  133.5 8.7 %fusion.16 = f32[4,64,512]{2,1,0:T(8,128)S(1)} fusion(bf16[4,4096,512]{2,1,0:T(8,128)(2,1)} %param.33, bf16[8,4,8,4096]{3,2,1,0:T(8,128)(2,1)S(1)} %all_to_all.36), kind=kOutput, calls=%fused_computation.14 | convolution fusion | flops 1073872896 | bytes 19398656 | tf_op jit(solution)/shard_map/erd,edf->erf/dot_general | solution.py:35
  142.3 17.8 %convolution_convert_fusion = bf16[4,64,4096]{2,1,0:T(8,128)(2,1)} fusion(bf16[4,512,4096]{2,1,0:T(8,128)(2,1)} %param.35, bf16[4,4096,512]{2,1,0:T(8,128)(2,1)} %param.34, f32[4,64,512]{2,1,0:T(8,128)S(1)} %fusion.16, bf16[8,4,8,4096]{3,2,1,0:T(8,128)(2,1)S(1)} %all_to_all.36), kind=kOutput, calls=%fused_computation | convolution fusion | flops 2149711872 | bytes 38273024 | tf_op jit(solution)/shard_map/erf,efd->erd/dot_general | solution.py:41
  160.1 3.2 %copy.68 = bf16[4,64,4096]{2,0,1:T(4,128)(2,1)S(1)} copy(bf16[4,64,4096]{2,1,0:T(8,128)(2,1)} %convolution_convert_fusion) | data formatting | bytes 4194304
  163.3 2.6 %copy.74 = bf16[8,8,4,4096]{3,1,2,0:T(8,128)(2,1)} copy(bf16[8,8,4,4096]{3,2,1,0:T(4,128)(2,1)S(1)} %bitcast.110) | data formatting | bytes 4194304
  165.9 33.6 %reduce-scatter.8.cloned.1.call-done = bf16[8,16384]{1,0:T(8,128)(2,1)} async-done(((bf16[64,16384]{1,0:T(8,128)(2,1)}), bf16[8,16384]{1,0:T(8,128)(2,1)}) %reduce-scatter.8.cloned.1.call-update) | async-done | bytes 262160
  199.5 1.8 reshape.177
  201.3 3.5 %all-to-all-start.2 = ((bf16[4,8,4096]{2,0,1:T(4,128)(2,1)}), bf16[4,8,4096]{2,0,1:T(4,128)(2,1)S(1)}, u32[]{:S(2)}, u32[]{:S(2)}) async-start(bf16[4,8,4096]{2,0,1:T(4,128)(2,1)} %bitcast.22), calls=%async_computation.3 | async-start | bytes 524288 | tf_op jit(solution)/shard_map/all_to_all | solution.py:150
  204.9 0.7 pad_maximum_fusion
  205.6 4.6 %all-to-all-done.2 = bf16[4,8,4096]{2,0,1:T(4,128)(2,1)S(1)} async-done(((bf16[4,8,4096]{2,0,1:T(4,128)(2,1)}), bf16[4,8,4096]{2,0,1:T(4,128)(2,1)S(1)}, u32[]{:S(2)}, u32[]{:S(2)}) %all-to-all-start.2) | async-done | bytes 262176 | tf_op jit(solution)/shard_map/all_to_all | solution.py:150
  210.2 0.3 copy.108
  210.6 0.9 fusion
  (48 shorter events, 1.9 us)
Async XLA Ops:
  7.2 29.0 %copy-start = (bf16[256,4096]{1,0:T(8,128)(2,1)S(1)}, bf16[256,4096]{1,0:T(8,128)(2,1)}, u32[]{:S(2)}) copy-start(bf16[256,4096]{1,0:T(8,128)(2,1)} %param.31) | copy-start | bytes 6291460
  7.2 62.7 %reduce-scatter.6.cloned.1.call-start = ((), (), s32[]{:S(2)}) async-start(), calls=%async_computation.5 | async-start | bytes 589824 | tf_op jit(solution)/shard_map/reduce_scatter | solution.py:126
  27.2 6.6 %copy-start.5 = (f32[64,256]{1,0:T(8,128)S(1)}, f32[64,256]{1,0:T(8,128)}, u32[]{:S(2)}) copy-start(f32[64,256]{1,0:T(8,128)} %param.19) | copy-start | bytes 196612
  33.9 3.6 %copy-start.4 = (f32[64,256]{1,0:T(8,128)}, f32[64,256]{1,0:T(8,128)S(1)}, u32[]{:S(2)}) copy-start(f32[64,256]{1,0:T(8,128)S(1)} %fusion.49) | copy-start | bytes 196612
  36.1 1.4 copy-start.7
  36.1 2.1 copy-start.6
  36.1 2.1 copy-start.9
  36.1 33.8 %copy-start.2 = (bf16[8,4096]{1,0:T(8,128)(2,1)S(1)}, bf16[8,4096]{1,0:T(8,128)(2,1)}, u32[]{:S(2)}) copy-start(bf16[8,4096]{1,0:T(8,128)(2,1)} %param.18) | copy-start | bytes 196612
  37.4 162.1 %reduce-scatter.8.cloned.1.call-start = ((), (), s32[]{:S(2)}) async-start(), calls=%async_computation.6 | async-start | bytes 2359296
  165.9 39.0 %slice-start = ((bf16[64,3,256]{2,0,1:T(8,128)(2,1)}), bf16[64,2,256]{2,0,1:T(8,128)(2,1)S(1)}, s32[]{:S(2)}) async-start(bf16[64,3,256]{2,0,1:T(8,128)(2,1)} %param.20), calls=%async_computation.7 | async-start | bytes 131072 | tf_op jit(solution)/shard_map/slice | solution.py:92
  165.9 39.6 %copy-start.8 = (f32[8,4]{0,1:T(4,128)S(1)}, f32[8,4]{0,1:T(4,128)}, u32[]{:S(2)}) copy-start(f32[8,4]{0,1:T(4,128)} %param.22) | copy-start | bytes 388
  165.9 45.6 %copy-start.1 = (bf16[256,4096]{1,0:T(8,128)(2,1)S(1)}, bf16[256,4096]{1,0:T(8,128)(2,1)}, u32[]{:S(2)}) copy-start(bf16[256,4096]{1,0:T(8,128)(2,1)} %param.31) | copy-start | bytes 6291460
  165.9 44.7 %copy-start.3 = (bf16[8,4096]{1,0:T(8,128)(2,1)S(1)}, bf16[8,4096]{1,0:T(8,128)(2,1)}, u32[]{:S(2)}) copy-start(bf16[8,4096]{1,0:T(8,128)(2,1)} %reduce-scatter.6.cloned.1.call-done) | copy-start | bytes 196612
  201.3 8.9 %all-to-all-start.2 = ((bf16[4,8,4096]{2,0,1:T(4,128)(2,1)}), bf16[4,8,4096]{2,0,1:T(4,128)(2,1)S(1)}, u32[]{:S(2)}, u32[]{:S(2)}) async-start(bf16[4,8,4096]{2,0,1:T(4,128)(2,1)} %bitcast.22), calls=%async_computation.3 | async-start | bytes 524288 | tf_op jit(solution)/shard_map/all_to_all | solution.py:150
Sparse Core Ops, SparseCore 0:
  37.6 32.2 reduce-scatter.5
  166.0 33.4 reduce-scatter.7
